TPU v7x, 32 devices: a whole 2x2x4 slice. The times are simulated.
32 devices in a mesh: sp: 4 (over z), dp: 8 (over y, x, core).
Axes of the slice: x: 2, y: 2, z: 4, core: 2. Of those that a mesh axis runs over, the one named last changes fastest.
Arguments:
- queries: bfloat16 [8, 768, 6144], P('dp', None, 'sp'), may hold values from -64 to 64
- out_grad: bfloat16 [8, 768, 4096], P('dp', None, 'sp'), may hold values from -6 to 6
- latent: bfloat16 [8, 768, 512], P('dp'), may hold values from -6 to 6
- rope_key: bfloat16 [8, 768, 64], P('dp'), may hold values from -6 to 6
- kv_gain: float32 [512], replicated, may hold values from 0.1 to 1.9
- key_up: bfloat16 [512, 4096], P('dp', 'sp'), may hold values from -0.25 to 0.25
- value_up: bfloat16 [512, 4096], P('dp', 'sp'), may hold values from -0.25 to 0.25
Outputs:
- query_grad: bfloat16 [8, 768, 6144], P('dp', None, 'sp')
- latent_grad: bfloat16 [8, 768, 512], P('dp')
- rope_key_grad: bfloat16 [8, 768, 64], P('dp')
- key_up_grad: float32 [512, 4096], P('dp', 'sp')
- value_up_grad: float32 [512, 4096], P('dp', 'sp')
All inputs are finite; a program needn't handle non-finite values.
Results may differ from a plain program's by a relative error of at most 0.019.
The roundings to bfloat16 on the way count: a program that leaves them out, or rounds other values in their place, can miss the bound.
Values may be sent and summed in bfloat16 or wider, within the bound.
A program may use at most 64 MiB of HBM per device.

v0:
```python
import jax
import jax.numpy as jnp
from jax import lax
from jax.sharding import PartitionSpec as P

NOPE_DIM = 128
ROPE_DIM = 64
VALUE_DIM = 128
norm_eps = 1e-06
rope_theta = 10000.0


def rope_tables(length, width):
    half_width = width // 2
    frequency = rope_theta ** (-(jnp.arange(half_width, dtype=jnp.float32) * 2.0 / width))
    position = jnp.arange(length, dtype=jnp.int32).astype(jnp.float32)
    angles = position[:, None] * frequency[None, :]
    return (jnp.cos(angles), jnp.sin(angles))


def rotate(tensor, cosine, sine_table):
    half_width = tensor.shape[-1] // 2
    first_half = tensor[..., :half_width]
    second = tensor[..., half_width:]
    return jnp.concatenate(
        [first_half * cosine - second * sine_table, second * cosine + first_half * sine_table],
        axis=-1,
    )


def unrotate(upstream, cosine, sine_table):
    half_width = upstream.shape[-1] // 2
    first_half = upstream[..., :half_width]
    second = upstream[..., half_width:]
    return jnp.concatenate(
        [first_half * cosine + second * sine_table, second * cosine - first_half * sine_table],
        axis=-1,
    )


def head_backward(query_used, key_used, head_value, head_grad, score_scale):
    length = query_used.shape[0]
    scores = jnp.dot(query_used, key_used.T, preferred_element_type=jnp.float32) * score_scale
    causal = lax.broadcasted_iota(jnp.int32, (length, length), 0) >= lax.broadcasted_iota(
        jnp.int32, (length, length), 1
    )
    scores = jnp.where(causal, scores, -jnp.inf)
    row_top = jnp.max(scores, axis=1, keepdims=True)
    weights = jnp.exp(scores - row_top)
    probs = weights / jnp.sum(weights, axis=1, keepdims=True)
    probs_low = probs.astype(jnp.bfloat16)
    value_grad = jnp.dot(probs_low.T, head_grad, preferred_element_type=jnp.float32).astype(
        jnp.bfloat16
    )
    prob_grad = jnp.dot(head_grad, head_value.T, preferred_element_type=jnp.float32)
    center = jnp.sum(probs * prob_grad, axis=1, keepdims=True)
    score_grad = (probs * (prob_grad - center) * score_scale).astype(jnp.bfloat16)
    query_grad = jnp.dot(score_grad, key_used, preferred_element_type=jnp.float32)
    key_grad = jnp.dot(score_grad.T, query_used, preferred_element_type=jnp.float32)
    return (query_grad, key_grad, value_grad)


def attend(queries, head_grads, keys, values, key_rot, cosine, sine_table):
    length = queries.shape[0]
    head_count = head_grads.shape[1] // VALUE_DIM
    qk_width = NOPE_DIM + ROPE_DIM
    query_heads = queries.reshape(length, head_count, qk_width)
    rotated = rotate(
        query_heads[:, :, NOPE_DIM:].astype(jnp.float32), cosine[:, None, :], sine_table[:, None, :]
    ).astype(jnp.bfloat16)
    query_used = jnp.concatenate([query_heads[:, :, :NOPE_DIM], rotated], axis=-1).transpose(
        1, 0, 2
    )
    key_heads = keys.reshape(length, head_count, NOPE_DIM).transpose(1, 0, 2)
    key_used = jnp.concatenate(
        [key_heads, jnp.broadcast_to(key_rot[None], (head_count, length, ROPE_DIM))], axis=-1
    )
    value_heads = values.reshape(length, head_count, VALUE_DIM).transpose(1, 0, 2)
    grad_heads = head_grads.reshape(length, head_count, VALUE_DIM).transpose(1, 0, 2)
    score_scale = qk_width ** (-0.5)
    query_part, key_part, value_part = lax.map(
        lambda items: head_backward(items[0], items[1], items[2], items[3], score_scale),
        (query_used, key_used, value_heads, grad_heads),
    )
    query_rot_grad = unrotate(query_part[:, :, NOPE_DIM:], cosine[None], sine_table[None])
    query_grad = jnp.concatenate([query_part[:, :, :NOPE_DIM], query_rot_grad], axis=-1).astype(
        jnp.bfloat16
    )
    query_grad = query_grad.transpose(1, 0, 2).reshape(length, head_count * qk_width)
    key_plain_grad = (
        key_part[:, :, :NOPE_DIM]
        .astype(jnp.bfloat16)
        .transpose(1, 0, 2)
        .reshape(length, head_count * NOPE_DIM)
    )
    key_rot_grad = jnp.sum(key_part[:, :, NOPE_DIM:], axis=0)
    value_grad = value_part.transpose(1, 0, 2).reshape(length, head_count * VALUE_DIM)
    return (query_grad, key_plain_grad, key_rot_grad, value_grad)


def finish(comp_total, rot_total, raw_latent, inverse, kv_gain, cosine, sine_table):
    mixed = comp_total * kv_gain
    spread = jnp.mean(raw_latent * mixed, axis=-1, keepdims=True)
    latent_grad = (inverse * mixed - raw_latent * inverse**3 * spread).astype(jnp.bfloat16)
    rope_grad = unrotate(rot_total, cosine, sine_table).astype(jnp.bfloat16)
    return (latent_grad, rope_grad)


def shards(queries, out_grad, latent, rope_key, kv_gain, key_up, value_up):
    key_whole, value_whole = (
        lax.all_gather(key_up, "dp", axis=0, tiled=True),
        lax.all_gather(value_up, "dp", axis=0, tiled=True),
    )
    batch_count, seq_count, latent_width = latent.shape
    raw_latent = latent.astype(jnp.float32)
    inverse = lax.rsqrt(jnp.mean(raw_latent * raw_latent, axis=-1, keepdims=True) + norm_eps)
    compressed = (raw_latent * inverse * kv_gain).astype(jnp.bfloat16)
    cosine, sine_table = rope_tables(seq_count, ROPE_DIM)
    key_rot = rotate(rope_key.astype(jnp.float32), cosine, sine_table).astype(jnp.bfloat16)
    flat_comp = compressed.reshape(batch_count * seq_count, latent_width)
    keys = jnp.dot(flat_comp, key_whole, preferred_element_type=jnp.float32).astype(jnp.bfloat16)
    values = jnp.dot(flat_comp, value_whole, preferred_element_type=jnp.float32).astype(
        jnp.bfloat16
    )
    keys = keys.reshape(batch_count, seq_count, key_whole.shape[1])
    values = values.reshape(batch_count, seq_count, value_whole.shape[1])

    def per_sequence(items):
        query_grad, key_plain_grad, key_rot_grad, value_grad = attend(
            items[0], items[1], items[2], items[3], items[4], cosine, sine_table
        )
        comp_part = jnp.dot(
            key_plain_grad, key_whole.T, preferred_element_type=jnp.float32
        ) + jnp.dot(value_grad, value_whole.T, preferred_element_type=jnp.float32)
        return (query_grad, key_plain_grad, value_grad, comp_part, key_rot_grad)

    query_grad, key_plain_grad, value_grad, comp_part, rot_part = lax.map(
        per_sequence, (queries, out_grad, keys, values, key_rot)
    )
    grad_pair = jnp.concatenate([key_plain_grad, value_grad], axis=-1).reshape(
        batch_count * seq_count, -1
    )
    grad_scale = float(lax.axis_size("dp") * batch_count * seq_count) ** (-0.5)
    comp_total = lax.psum(comp_part.astype(jnp.bfloat16), "sp").astype(jnp.float32)
    rot_total = lax.psum(rot_part.astype(jnp.bfloat16), "sp").astype(jnp.float32)
    latent_grad, rope_grad = finish(
        comp_total, rot_total, raw_latent, inverse, kv_gain, cosine, sine_table
    )
    product = lax.dot_general(
        flat_comp, grad_pair, (((0,), (0,)), ((), ())), preferred_element_type=jnp.float32
    )
    combined = lax.psum_scatter(product * grad_scale, "dp", scatter_dimension=0, tiled=True)
    split_at = key_up.shape[1]
    return (query_grad, latent_grad, rope_grad, combined[:, :split_at], combined[:, split_at:])


def solution(mesh):
    return jax.shard_map(
        shards,
        mesh=mesh,
        in_specs=(
            P("dp", None, "sp"),
            P("dp", None, "sp"),
            P("dp", None, None),
            P("dp", None, None),
            P(),
            P("dp", "sp"),
            P("dp", "sp"),
        ),
        out_specs=(
            P("dp", None, "sp"),
            P("dp", None, None),
            P("dp", None, None),
            P("dp", "sp"),
            P("dp", "sp"),
        ),
        check_vma=False,
    )
```

profile of v0, /device:TPU:0, one launch (start us, length us, event | category | flops | bytes accessed | tf_op | source)
XLA Modules:
  0.0 271.9 jit_solution(8573621979364724312)
XLA Ops:
  10.3 2.6 copy.21
  12.9 2.8 %copy.18 = bf16[1,768,1536]{1,2,0:T(8,128)(2,1)S(1)} copy(bf16[1,768,1536]{2,1,0:T(8,128)(2,1)} %param.9) | data formatting | bytes 4718592 | tf_op args[0]
  15.9 1.0 copy-done
  18.2 1.6 maximum_bitcast_fusion.2
  19.8 16.2 %all-gather.5.cloned.1.call-done = bf16[512,1024]{1,0:T(8,128)(2,1)} async-done(((bf16[64,1024]{1,0:T(8,128)(2,1)}), bf16[512,1024]{1,0:T(8,128)(2,1)}) %all-gather.5.cloned.1.call-update) | async-done | bytes 1048592 | tf_op jit(solution)/shard_map/all_gather | solution.py:112
  36.0 2.3 fusion.43
  38.3 1.4 copy.35
  39.7 21.6 %all-gather.3.cloned.1.call-done = bf16[512,1024]{1,0:T(8,128)(2,1)} async-done(((bf16[64,1024]{1,0:T(8,128)(2,1)}), bf16[512,1024]{1,0:T(8,128)(2,1)}) %all-gather.3.cloned.1.call-update) | async-done | bytes 1048592 | tf_op jit(solution)/shard_map/all_gather | solution.py:111
  61.3 2.3 fusion.42
  64.0 2.3 pad_maximum_fusion
  66.4 88.8 %while.19 = (s32[]{:T(128)}, f32[8,768,192]{1,2,0:T(8,128)}, f32[8,768,192]{1,2,0:T(8,128)}, bf16[8,768,128]{1,2,0:T(8,128)(2,1)}, bf16[8,768,192]{1,2,0:T(8,128...) while((s32[]{:T(128)}, f32[8,768,192]{1,2,0:T(8,128)}, ...), condition=%wide.region_5.6_spmd, body=%wide.region_1.5_spmd.sunk | while | flops 992769792 | bytes 24220780 | solution.py:81
  66.4 1.6 fusion.96
  68.3 1.4 fusion.100
  70.6 1.6 multiply_reduce_fusion.2
  72.8 2.3 fusion.99
  75.2 2.3 fusion.98
  77.5 1.6 fusion.96
  79.4 1.4 fusion.100
  81.7 1.6 multiply_reduce_fusion.2
  83.9 2.4 fusion.99
  86.3 2.2 fusion.98
  88.5 1.6 fusion.96
  90.5 1.4 fusion.100
  92.8 1.6 multiply_reduce_fusion.2
  95.0 2.3 fusion.99
  97.3 2.3 fusion.98
  99.6 1.6 fusion.96
  101.6 1.4 fusion.100
  103.9 1.6 multiply_reduce_fusion.2
  106.1 2.4 fusion.99
  108.5 2.3 fusion.98
  110.7 1.6 fusion.96
  112.7 1.4 fusion.100
  115.0 1.6 multiply_reduce_fusion.2
  117.2 2.3 fusion.99
  119.5 2.3 fusion.98
  121.8 1.6 fusion.96
  123.8 1.4 fusion.100
  126.1 1.6 multiply_reduce_fusion.2
  128.3 2.4 fusion.99
  130.7 2.2 fusion.98
  132.9 1.6 fusion.96
  134.9 1.4 fusion.100
  137.2 1.6 multiply_reduce_fusion.2
  139.4 2.4 fusion.99
  141.8 2.3 fusion.98
  144.0 1.6 fusion.96
  146.0 1.4 fusion.100
  148.3 1.6 multiply_reduce_fusion.2
  150.5 2.4 fusion.99
  152.9 2.3 fusion.98
  155.1 2.2 slice_reduce_fusion
  157.4 2.1 slice.115
  159.5 1.0 fusion.70
  161.1 1.9 fusion.44
  163.3 5.5 %convolution_multiply_fusion = f32[512,2048]{1,0:T(8,128)} fusion(bf16[1,768,1024]{1,2,0:T(8,128)(2,1)} %bitcast.133, bf16[1,768,1024]{1,2,0:T(8,128)(2,1)S(1)} %bitcast.131, bf16[1,768,512]{2,1,0:T(8,128)(2,1)S(1)} %copy-done, f32[512]{0:T(512)S(1)} %copy-done.9, f32[768]{0:T(1024)S(1)} %copy-done.7), kind=kOutput, calls=%fused_computation.36 | convolution fusion | flops 1619525632 | bytes 8131584 | tf_op jit(solution)/shard_map/dot_general | solution.py:149
  168.9 2.1 slice.116
  171.0 1.6 add_convert_fusion.1
  172.8 2.4 copy.26
  175.2 34.8 %all-reduce.3.cloned.1.call-done = (bf16[1,768,512]{2,1,0:T(8,128)(2,1)}, bf16[1,768,64]{1,2,0:T(8,128)(2,1)}) async-done(((bf16[1,768,512]{2,1,0:T(8,128)(2,1)}, bf16[1,768,64]{1,2,0:T(8,128)(2,1)}), (bf16[1,768,512]{2,1,0:T(8,128)(2,1)}, bf16[1,768,64]{1,2,0:T(8,128)(2,1)})) %all-reduce.3.cloned.1.call-update) | async-done | bytes 884752 | tf_op jit(solution)/shard_map/psum | solution.py:144
  212.1 1.5 fusion.41
  213.6 1.3 fusion.40
  215.0 48.6 %reduce-scatter.2.cloned.1.call-done = f32[64,2048]{1,0:T(8,128)} async-done(((f32[512,2048]{1,0:T(8,128)}), f32[64,2048]{1,0:T(8,128)}) %reduce-scatter.2.cloned.1.call-update) | async-done | bytes 524304 | tf_op jit(solution)/shard_map/reduce_scatter | solution.py:152
  263.5 1.9 fusion.69
  (91 shorter events, 22.6 us)
Async XLA Ops:
  7.2 28.8 %all-gather.5.cloned.1.call-start = ((), (), s32[]{:S(2)}) async-start(), calls=%async_computation.2 | async-start | bytes 1179648 | tf_op jit(solution)/shard_map/all_gather | solution.py:112
  7.9 53.4 %all-gather.3.cloned.1.call-start = ((), (), s32[]{:S(2)}) async-start(), calls=%async_computation.1 | async-start | bytes 1179648 | tf_op jit(solution)/shard_map/all_gather | solution.py:111
  8.6 201.4 %all-reduce.3.cloned.1.call-start = ((), (), s32[]{:S(2)}) async-start(), calls=%async_computation.4 | async-start | bytes 1769472 | tf_op jit(solution)/shard_map/psum | solution.py:144
  8.7 8.4 %copy-start.10 = (f32[32]{0:T(128)}, f32[32]{0:T(128)S(1)}, u32[]{:S(2)}) copy-start(f32[32]{0:T(128)S(1)} %negate_power_fusion) | copy-start | bytes 388
  15.7 1.1 copy-start
  17.5 0.6 copy-start.2
  17.5 0.7 copy-start.4
  18.2 17.8 %copy-start.8 = (f32[512]{0:T(512)S(1)}, f32[512]{0:T(512)}, u32[]{:S(2)}) copy-start(f32[512]{0:T(512)} %param.13) | copy-start | bytes 6148
  19.8 41.5 %copy-start.6 = (f32[768]{0:T(1024)}, f32[768]{0:T(1024)S(1)}, u32[]{:S(2)}) copy-start(f32[768]{0:T(1024)S(1)} %get-tuple-element.145) | copy-start | bytes 9220
  155.1 4.3 %copy-start.14 = (bf16[512,1024]{1,0:T(8,128)(2,1)S(1)}, bf16[512,1024]{1,0:T(8,128)(2,1)}, u32[]{:S(2)}) copy-start(bf16[512,1024]{1,0:T(8,128)(2,1)} %all-gather.3.cloned.1.call-done) | copy-start | bytes 3145732
  159.4 1.4 copy-start.12
  159.4 1.7 copy-start.13
  161.1 2.2 copy-start.7
  161.1 2.2 copy-start.9
  163.1 100.4 %reduce-scatter.2.cloned.1.call-start = ((), (), s32[]{:S(2)}) async-start(), calls=%async_computation.3 | async-start | bytes 4718592 | tf_op jit(solution)/shard_map/reduce_scatter | solution.py:152
  168.9 2.1 copy-start.3
  168.9 2.1 copy-start.5
  172.8 38.3 %copy-start.11 = (f32[32]{0:T(128)S(1)}, f32[32]{0:T(128)}, u32[]{:S(2)}) copy-start(f32[32]{0:T(128)} %copy-done.10) | copy-start | bytes 388
  210.1 3.6 %copy-start.1 = (bf16[1,768,512]{2,1,0:T(8,128)(2,1)S(1)}, bf16[1,768,512]{2,1,0:T(8,128)(2,1)}, u32[]{:S(2)}) copy-start(bf16[1,768,512]{2,1,0:T(8,128)(2,1)} %get-tuple-element.126) | copy-start | bytes 2359300
Sparse Core Ops, SparseCore 0:
  9.9 26.0 all-gather.4
  37.9 23.3 all-gather.2
  163.2 46.8 all-reduce.2
  213.3 50.2 reduce-scatter.1
where the time goes:
time: 274 us; the launch traced here: 272 us
  waiting for transfers between devices  123 us (45%)
  matrix products  87 us (32%)
  local copies, waits for them, and re-layouts  24.8 us (9%)
  other arithmetic  22.9 us (8%)
  between operations  14.1 us (5%)
    reduce_scatter x1, waiting for transfers between devices, shards(): lax.psum_scatter(product * grad_scale, 'dp', scatter_dimension=0, tiled=T...  48.6 us
    psum x1, waiting for transfers between devices, shards(): lax.psum(comp_part.astype(jnp.bfloat16), 'sp').astype(jnp.float32)  34.8 us
    all_gather x1, waiting for transfers between devices, shards(): lax.all_gather(key_up, 'dp', axis=0, tiled=True)  21.6 us
    dot_general x8, matrix products, head_backward(): jnp.dot(score_grad.T, query_used, preferred_element_type=jnp.float32)  18.9 us
    dot_general x8, matrix products, head_backward(): jnp.dot(score_grad, key_used, preferred_element_type=jnp.float32)  18.1 us
    all_gather x1, waiting for transfers between devices, shards(): lax.all_gather(value_up, 'dp', axis=0, tiled=True)  16.2 us
    dot_general x8, matrix products, head_backward(): jnp.dot(head_grad, head_value.T, preferred_element_type=jnp.float32)  12.8 us
    dot_general x8, matrix products, head_backward(): jnp.dot(query_used, key_used.T, preferred_element_type=jnp.float32)  12.7 us
  transfers between devices with their start and end apart: 4, of which 4 were waited for; matrix products, arithmetic and copies ran while one was open for 11% of the time, Pallas kernels for 0%

commit v1 on v0

--- a/solution.py
+++ b/solution.py
@@ -8,6 +8,12 @@
 VALUE_DIM = 128
 norm_eps = 1e-06
 rope_theta = 10000.0
+
+
+def gather_and_add(block, axis):
+    terms = lax.all_gather(block, axis, axis=0, tiled=False)
+    total = terms.sum(axis=0)
+    return total
 
 
 def rope_tables(length, width):
@@ -141,7 +147,7 @@
         batch_count * seq_count, -1
     )
     grad_scale = float(lax.axis_size("dp") * batch_count * seq_count) ** (-0.5)
-    comp_total = lax.psum(comp_part.astype(jnp.bfloat16), "sp").astype(jnp.float32)
+    comp_total = gather_and_add(comp_part.astype(jnp.bfloat16), "sp").astype(jnp.float32)
     rot_total = lax.psum(rot_part.astype(jnp.bfloat16), "sp").astype(jnp.float32)
     latent_grad, rope_grad = finish(
         comp_total, rot_total, raw_latent, inverse, kv_gain, cosine, sine_table

time: 274 us -> 322 us (1.18)
  waiting for transfers between devices: 123 us -> 170 us
    all_gather x0 -> x1, waiting for transfers between devices: none -> 63.2 us  [gather_and_add(): terms = lax.all_gather(block, axis, axis=0, tiled=False)]
    psum x1, waiting for transfers between devices: 34.8 us -> 18.8 us  [shards(): lax.psum(rot_part.astype(jnp.bfloat16), 'sp').astype(jnp.float32)]
    unnamed x33 -> x31, local copies, waits for them, and re-layouts: 9.88 us -> 9.88 us
  transfers between devices with their start and end apart: 4 -> 5, of which waited for: 4 -> 5; matrix products, arithmetic and copies ran while one was open for 11% -> 11% of each run, Pallas kernels for 0% -> 0%
where the time goes in v1:
time: 322 us; the launch traced here: 321 us
  waiting for transfers between devices  170 us (53%)
  matrix products  87 us (27%)
  local copies, waits for them, and re-layouts  24.8 us (8%)
  other arithmetic  24.5 us (8%)
  between operations  14.1 us (4%)
    all_gather x1, waiting for transfers between devices, gather_and_add(): terms = lax.all_gather(block, axis, axis=0, tiled=False)  63.2 us
    reduce_scatter x1, waiting for transfers between devices, shards(): lax.psum_scatter(product * grad_scale, 'dp', scatter_dimension=0, tiled=T...  48.5 us
    all_gather x1, waiting for transfers between devices, shards(): lax.all_gather(key_up, 'dp', axis=0, tiled=True)  21.6 us
    dot_general x8, matrix products, head_backward(): jnp.dot(score_grad.T, query_used, preferred_element_type=jnp.float32)  19 us
    psum x1, waiting for transfers between devices, shards(): lax.psum(rot_part.astype(jnp.bfloat16), 'sp').astype(jnp.float32)  18.8 us
    dot_general x8, matrix products, head_backward(): jnp.dot(score_grad, key_used, preferred_element_type=jnp.float32)  18 us
    all_gather x1, waiting for transfers between devices, shards(): lax.all_gather(value_up, 'dp', axis=0, tiled=True)  16.2 us
    dot_general x8, matrix products, head_backward(): jnp.dot(head_grad, head_value.T, preferred_element_type=jnp.float32)  12.8 us
  transfers between devices with their start and end apart: 5, of which 5 were waited for; matrix products, arithmetic and copies ran while one was open for 11% of the time, Pallas kernels for 0%

profile of v1, /device:TPU:0, one launch (start us, length us, event | category | flops | bytes accessed | tf_op | source)
XLA Modules:
  0.0 320.8 jit_solution(13778856997985525466)
XLA Ops:
  10.3 2.6 copy.21
  12.9 2.8 copy.18
  18.2 1.6 maximum_bitcast_fusion.2
  19.8 16.2 %all-gather.7.cloned.1.call-done = bf16[512,1024]{1,0:T(8,128)(2,1)} async-done(((bf16[64,1024]{1,0:T(8,128)(2,1)}), bf16[512,1024]{1,0:T(8,128)(2,1)}) %all-gather.7.cloned.1.call-update) | async-done | bytes 1048592 | tf_op jit(solution)/shard_map/all_gather | solution.py:118
  36.0 2.3 fusion.44
  38.3 1.4 copy.36
  39.7 21.6 %all-gather.5.cloned.1.call-done = bf16[512,1024]{1,0:T(8,128)(2,1)} async-done(((bf16[64,1024]{1,0:T(8,128)(2,1)}), bf16[512,1024]{1,0:T(8,128)(2,1)}) %all-gather.5.cloned.1.call-update) | async-done | bytes 1048592 | tf_op jit(solution)/shard_map/all_gather | solution.py:117
  61.3 2.3 fusion.43
  64.0 2.3 pad_maximum_fusion
  66.4 88.8 %while.19 = (s32[]{:T(128)}, f32[8,768,192]{1,2,0:T(8,128)}, f32[8,768,192]{1,2,0:T(8,128)}, bf16[8,768,128]{1,2,0:T(8,128)(2,1)}, bf16[8,768,192]{1,2,0:T(8,128...) while((s32[]{:T(128)}, f32[8,768,192]{1,2,0:T(8,128)}, ...), condition=%wide.region_5.6_spmd, body=%wide.region_1.5_spmd.sunk | while | flops 992769792 | bytes 24220780 | solution.py:87
  66.4 1.6 fusion.96
  68.3 1.4 fusion.100
  70.6 1.6 multiply_reduce_fusion.2
  72.8 2.3 fusion.99
  75.2 2.3 fusion.98
  77.4 1.6 fusion.96
  79.4 1.4 fusion.100
  81.7 1.6 multiply_reduce_fusion.2
  83.9 2.4 fusion.99
  86.3 2.3 fusion.98
  88.5 1.6 fusion.96
  90.5 1.4 fusion.100
  92.8 1.6 multiply_reduce_fusion.2
  95.0 2.4 fusion.99
  97.4 2.3 fusion.98
  99.6 1.6 fusion.96
  101.6 1.4 fusion.100
  103.9 1.6 multiply_reduce_fusion.2
  106.1 2.4 fusion.99
  108.5 2.2 fusion.98
  110.7 1.6 fusion.96
  112.7 1.4 fusion.100
  115.0 1.6 multiply_reduce_fusion.2
  117.2 2.3 fusion.99
  119.6 2.3 fusion.98
  121.8 1.6 fusion.96
  123.8 1.4 fusion.100
  126.1 1.6 multiply_reduce_fusion.2
  128.3 2.4 fusion.99
  130.7 2.2 fusion.98
  132.9 1.6 fusion.96
  134.9 1.4 fusion.100
  137.2 1.6 multiply_reduce_fusion.2
  139.4 2.4 fusion.99
  141.8 2.2 fusion.98
  144.0 1.6 fusion.96
  146.0 1.4 fusion.100
  148.3 1.6 multiply_reduce_fusion.2
  150.5 2.4 fusion.99
  152.9 2.3 fusion.98
  155.1 2.2 slice_reduce_fusion
  157.4 2.1 slice.115
  159.5 1.0 fusion.70
  161.2 1.9 add_convert_fusion
  163.4 5.5 %convolution_multiply_fusion = f32[512,2048]{1,0:T(8,128)} fusion(bf16[1,768,1024]{1,2,0:T(8,128)(2,1)} %bitcast.137, bf16[1,768,1024]{1,2,0:T(8,128)(2,1)S(1)} %bitcast.135, bf16[1,768,512]{2,1,0:T(8,128)(2,1)S(1)} %copy-done, f32[512]{0:T(512)S(1)} %copy-done.8, f32[768]{0:T(1024)S(1)} %copy-done.6), kind=kOutput, calls=%fused_computation.36 | convolution fusion | flops 1619525632 | bytes 8131584 | tf_op jit(solution)/shard_map/dot_general | solution.py:155
  169.0 2.1 slice.116
  171.1 1.6 add_convert_fusion.1
  172.9 2.4 copy.26
  175.3 18.8 %all-reduce.2.cloned.1.call-done = bf16[1,768,64]{1,2,0:T(8,128)(2,1)} async-done(((bf16[1,768,64]{1,2,0:T(8,128)(2,1)}), bf16[1,768,64]{1,2,0:T(8,128)(2,1)}) %all-reduce.2.cloned.1.call-update) | async-done | bytes 98320 | tf_op jit(solution)/shard_map/psum | solution.py:151
  196.1 63.2 %all-gather.9.cloned.1.call-done = bf16[3072,512]{1,0:T(8,128)(2,1)} async-done(((bf16[768,512]{1,0:T(8,128)(2,1)}), bf16[3072,512]{1,0:T(8,128)(2,1)}) %all-gather.9.cloned.1.call-update) | async-done | bytes 3145744 | tf_op jit(solution)/shard_map/all_gather | solution.py:14
  259.3 2.8 reduce.4
  262.5 1.3 fusion.40
  263.8 48.5 %reduce-scatter.2.cloned.1.call-done = f32[64,2048]{1,0:T(8,128)} async-done(((f32[512,2048]{1,0:T(8,128)}), f32[64,2048]{1,0:T(8,128)}) %reduce-scatter.2.cloned.1.call-update) | async-done | bytes 524304 | tf_op jit(solution)/shard_map/reduce_scatter | solution.py:158
  312.4 1.9 fusion.69
  (93 shorter events, 23.9 us)
Async XLA Ops:
  7.2 28.8 %all-gather.7.cloned.1.call-start = ((), (), s32[]{:S(2)}) async-start(), calls=%async_computation.2 | async-start | bytes 1179648 | tf_op jit(solution)/shard_map/all_gather | solution.py:118
  7.9 53.4 %all-gather.5.cloned.1.call-start = ((), (), s32[]{:S(2)}) async-start(), calls=%async_computation.1 | async-start | bytes 1179648 | tf_op jit(solution)/shard_map/all_gather | solution.py:117
  8.6 185.5 %all-reduce.2.cloned.1.call-start = ((), (), s32[]{:S(2)}) async-start(), calls=%async_computation.3 | async-start | bytes 196608 | tf_op jit(solution)/shard_map/psum | solution.py:151
  8.7 8.4 %copy-start.9 = (f32[32]{0:T(128)}, f32[32]{0:T(128)S(1)}, u32[]{:S(2)}) copy-start(f32[32]{0:T(128)S(1)} %negate_power_fusion) | copy-start | bytes 388
  15.7 1.1 copy-start
  17.5 0.6 copy-start.1
  17.5 0.7 copy-start.3
  18.2 17.8 %copy-start.7 = (f32[512]{0:T(512)S(1)}, f32[512]{0:T(512)}, u32[]{:S(2)}) copy-start(f32[512]{0:T(512)} %param.13) | copy-start | bytes 6148
  19.8 41.5 %copy-start.5 = (f32[768]{0:T(1024)}, f32[768]{0:T(1024)S(1)}, u32[]{:S(2)}) copy-start(f32[768]{0:T(1024)S(1)} %get-tuple-element.143) | copy-start | bytes 9220
  155.1 4.4 %copy-start.13 = (bf16[512,1024]{1,0:T(8,128)(2,1)S(1)}, bf16[512,1024]{1,0:T(8,128)(2,1)}, u32[]{:S(2)}) copy-start(bf16[512,1024]{1,0:T(8,128)(2,1)} %all-gather.5.cloned.1.call-done) | copy-start | bytes 3145732
  159.5 99.9 %all-gather.9.cloned.1.call-start = ((), (), s32[]{:S(2)}) async-start(), calls=%async_computation.5 | async-start | bytes 3932160 | tf_op jit(solution)/shard_map/all_gather | solution.py:14
  159.5 1.4 copy-start.11
  159.5 1.7 copy-start.12
  161.2 2.2 copy-start.6
  161.2 2.2 copy-start.8
  163.2 149.2 %reduce-scatter.2.cloned.1.call-start = ((), (), s32[]{:S(2)}) async-start(), calls=%async_computation.4 | async-start | bytes 4718592 | tf_op jit(solution)/shard_map/reduce_scatter | solution.py:158
  169.0 2.1 copy-start.2
  169.0 2.1 copy-start.4
  172.9 22.1 %copy-start.10 = (f32[32]{0:T(128)S(1)}, f32[32]{0:T(128)}, u32[]{:S(2)}) copy-start(f32[32]{0:T(128)} %copy-done.9) | copy-start | bytes 388
Sparse Core Ops, SparseCore 0:
  9.9 26.0 all-gather.6
  37.9 23.3 all-gather.4
  159.6 34.4 all-reduce.1
  196.1 63.1 all-gather.8
  262.5 49.7 reduce-scatter.1
